TPU v7x, 32 devices: a whole 2x2x4 slice. The times are simulated.
32 devices in a mesh: fs: 8 (over z, y), tp: 4 (over x, core).
Axes of the slice: x: 2, y: 2, z: 4, core: 2. Of those that a mesh axis runs over, the one named last changes fastest.
Arguments:
- tokens: bfloat16 [8192, 2048], P(('fs', 'tp')), may hold values from -6 to 6
- first_block_norm_scale: float32 [2048], replicated, may hold values from 0.1 to 1.9
- first_block_gate_matrix: bfloat16 [2048, 5504], P('fs', 'tp'), may hold values from -0.125 to 0.125
- first_block_up_matrix: bfloat16 [2048, 5504], P('fs', 'tp'), may hold values from -0.125 to 0.125
- first_block_down_matrix: bfloat16 [5504, 2048], P('tp', 'fs'), may hold values from -0.078125 to 0.078125
- mixer_norm_scale: float32 [2048], replicated, may hold values from 0.1 to 1.9
- recurrent_input_matrix: bfloat16 [2048, 3072], P('fs', 'tp'), may hold values from -0.125 to 0.125
- output_gate_projection: bfloat16 [2048, 3072], P('fs', 'tp'), may hold values from -0.125 to 0.125
- convolution_kernel: float32 [4, 3072], P(None, 'tp'), may hold values from -2 to 2
- decay_gate_blocks: bfloat16 [16, 192, 192], P('tp'), may hold values from -0.4375 to 0.4375
- input_gate_blocks: bfloat16 [16, 192, 192], P('tp'), may hold values from -0.4375 to 0.4375
- channel_decay_weight: float32 [3072], P('tp'), may hold values from 3.5 to 11.5
- position_decay_extra: float32 [8192], P('fs'), may hold values from -0.7 to 0
- mixer_output_matrix: bfloat16 [3072, 2048], P('tp', 'fs'), may hold values from -0.109375 to 0.109375
- second_block_norm_scale: float32 [2048], replicated, may hold values from 0.1 to 1.9
- second_block_gate_matrix: bfloat16 [2048, 5504], P('fs', 'tp'), may hold values from -0.125 to 0.125
- second_block_up_matrix: bfloat16 [2048, 5504], P('fs', 'tp'), may hold values from -0.125 to 0.125
- second_block_down_matrix: bfloat16 [5504, 2048], P('tp', 'fs'), may hold values from -0.078125 to 0.078125
Outputs:
- layer_out: bfloat16 [8192, 2048], P(('fs', 'tp'))
All inputs are finite; a program needn't handle non-finite values.
Results may differ from a plain program's by a relative error of at most 0.019.
Values may be sent and summed in bfloat16 or wider, within the bound.
A program may use at most 128 MiB of HBM per device.

v0:
```python
import jax
import jax.numpy as jnp
from jax import lax
from jax.sharding import PartitionSpec as P

EPS = 1e-06
RECURRENT_WIDTH = 8.0


def normed(input_token_rows, norm_scale_vector):
    values = input_token_rows.astype(jnp.float32)
    square = jnp.mean(values * values, axis=-1, keepdims=True)
    return (values * lax.rsqrt(square + EPS) * norm_scale_vector).astype(jnp.bfloat16)


def combine(earlier, later):
    decay_one, drive_one = earlier
    decay_two, drive_two = later
    return (decay_one * decay_two, decay_two * drive_one + drive_two)


def sublayer(
    residual_activations,
    norm_scale_vector,
    first_weight,
    second_weight,
    out_weight,
    middle,
    sequence,
    row_count,
):
    normal = normed(residual_activations, norm_scale_vector)
    whole = lax.all_gather(normal, "tp", axis=0, tiled=True)
    empty = jnp.zeros((whole.shape[0], first_weight.shape[1]), jnp.float32)
    totals = (empty, empty)
    pieces = (
        lax.all_gather(first_weight, "fs", axis=0, tiled=True),
        lax.all_gather(second_weight, "fs", axis=0, tiled=True),
    )
    columns = lax.slice_in_dim(whole, 0, pieces[0].shape[0], axis=1)
    totals = (
        totals[0] + jnp.dot(columns, pieces[0], preferred_element_type=jnp.float32),
        totals[1] + jnp.dot(columns, pieces[1], preferred_element_type=jnp.float32),
    )
    projected = middle(totals[0], totals[1])
    if sequence is not None:
        projected = sequence(projected)
    full_out = lax.all_gather(out_weight, "fs", axis=1, tiled=True)
    picked = lax.slice_in_dim(projected, 0, row_count * lax.axis_size("tp"), axis=0)
    return lax.psum_scatter(
        jnp.dot(picked, full_out, preferred_element_type=jnp.float32).astype(jnp.bfloat16),
        "tp",
        scatter_dimension=0,
        tiled=True,
    ).astype(jnp.float32)


def shards(
    tokens,
    first_block_norm_scale,
    first_block_gate_matrix,
    first_block_up_matrix,
    first_block_down_matrix,
    mixer_norm_scale,
    recurrent_input_matrix,
    output_gate_projection,
    convolution_kernel,
    decay_gate_blocks,
    input_gate_blocks,
    channel_decay_weight,
    position_decay_extra,
    mixer_output_matrix,
    second_block_norm_scale,
    second_block_gate_matrix,
    second_block_up_matrix,
    second_block_down_matrix,
):
    row_count = tokens.shape[0]
    residual_activations = tokens

    def feed_middle(gate_pre, up_pre):
        return (jax.nn.silu(gate_pre) * up_pre).astype(jnp.bfloat16)

    def mixer_middle(recur_pre, branch_pre):
        return jnp.concatenate(
            [recur_pre.astype(jnp.bfloat16), branch_pre.astype(jnp.bfloat16)], axis=1
        )

    def recurrent(projected):
        channels = projected.shape[1] // 2
        length = projected.shape[0]
        recur_rows = projected[:, :channels]
        branch_rows = projected[:, channels:]
        taps = convolution_kernel.shape[0]
        summed = lax.conv_general_dilated(
            recur_rows.astype(jnp.float32)[None],
            convolution_kernel[:, None, :],
            window_strides=(1,),
            padding=((taps - 1, 0),),
            dimension_numbers=("NWC", "WIO", "NWC"),
            feature_group_count=channels,
            precision=lax.Precision.HIGHEST,
        )[0]
        conv_out = summed.astype(jnp.bfloat16)
        grouped = conv_out.reshape(length, decay_gate_blocks.shape[0], decay_gate_blocks.shape[1])
        decay_gate_value = jax.nn.sigmoid(
            jnp.einsum(
                "thi,hij->thj", grouped, decay_gate_blocks, preferred_element_type=jnp.float32
            ).reshape(length, channels)
        )
        input_gate = jax.nn.sigmoid(
            jnp.einsum(
                "thi,hij->thj", grouped, input_gate_blocks, preferred_element_type=jnp.float32
            ).reshape(length, channels)
        )
        log_decay_factor = (
            -RECURRENT_WIDTH * decay_gate_value * jax.nn.softplus(-channel_decay_weight)
            + position_decay_extra[:, None]
        )
        decay_rate = jnp.exp(log_decay_factor)
        drive_in = (
            jnp.sqrt(-jnp.expm1(2.0 * log_decay_factor)) * input_gate * conv_out.astype(jnp.float32)
        )
        _, hidden_state = lax.associative_scan(combine, (decay_rate, drive_in), axis=0)
        return (
            jax.nn.gelu(branch_rows.astype(jnp.float32), approximate=True) * hidden_state
        ).astype(jnp.bfloat16)

    first_out = sublayer(
        residual_activations,
        first_block_norm_scale,
        first_block_gate_matrix,
        first_block_up_matrix,
        first_block_down_matrix,
        feed_middle,
        None,
        row_count,
    )
    residual_activations = (residual_activations.astype(jnp.float32) + 0.5 * first_out).astype(
        jnp.bfloat16
    )
    mixer_output_rows = sublayer(
        residual_activations,
        mixer_norm_scale,
        recurrent_input_matrix,
        output_gate_projection,
        mixer_output_matrix,
        mixer_middle,
        recurrent,
        row_count,
    )
    residual_activations = (residual_activations.astype(jnp.float32) + mixer_output_rows).astype(
        jnp.bfloat16
    )
    second_out = sublayer(
        residual_activations,
        second_block_norm_scale,
        second_block_gate_matrix,
        second_block_up_matrix,
        second_block_down_matrix,
        feed_middle,
        None,
        row_count,
    )
    residual_activations = (residual_activations.astype(jnp.float32) + 0.5 * second_out).astype(
        jnp.bfloat16
    )
    return residual_activations


def solution(mesh):
    in_specs = (
        P(("fs", "tp"), None),
        P(),
        P("fs", "tp"),
        P("fs", "tp"),
        P("tp", "fs"),
        P(),
        P("fs", "tp"),
        P("fs", "tp"),
        P(None, "tp"),
        P("tp", None, None),
        P("tp", None, None),
        P("tp"),
        P("fs"),
        P("tp", "fs"),
        P(),
        P("fs", "tp"),
        P("fs", "tp"),
        P("tp", "fs"),
    )
    out_specs = P(("fs", "tp"), None)
    return jax.shard_map(shards, mesh=mesh, in_specs=in_specs, out_specs=out_specs, check_vma=False)
```

profile of v0, /device:TPU:0, one launch (start us, length us, event | category | flops | bytes accessed | tf_op | source)
XLA Modules:
  0.0 1164.1 jit_solution(1471374733268699723)
XLA Ops:
  8.1 2.5 fusion.11
  12.8 35.2 %all-gather.13.cloned.1.call-done = bf16[1024,2048]{1,0:T(8,128)(2,1)} async-done(((bf16[256,2048]{1,0:T(8,128)(2,1)}), bf16[1024,2048]{1,0:T(8,128)(2,1)}) %all-gather.13.cloned.1.call-update) | async-done | bytes 4194320 | tf_op jit(solution)/shard_map/all_gather | solution.py:33
  48.0 93.6 %all-gather.15.cloned.1.call-done = bf16[2048,1376]{0,1:T(8,128)(2,1)} async-done(((bf16[256,1376]{0,1:T(8,128)(2,1)}), bf16[2048,1376]{0,1:T(8,128)(2,1)}) %all-gather.15.cloned.1.call-update) | async-done | bytes 5636112 | tf_op jit(solution)/shard_map/all_gather | solution.py:37
  141.6 10.8 fusion.65
  152.4 81.0 %all-gather.17.cloned.1.call-done = bf16[2048,1376]{0,1:T(8,128)(2,1)} async-done(((bf16[256,1376]{0,1:T(8,128)(2,1)}), bf16[2048,1376]{0,1:T(8,128)(2,1)}) %all-gather.17.cloned.1.call-update) | async-done | bytes 5636112 | tf_op jit(solution)/shard_map/all_gather | solution.py:38
  233.4 91.7 %all-gather.19.cloned.1.call-done = bf16[1376,2048]{1,0:T(8,128)(2,1)} async-done(((bf16[1376,256]{1,0:T(8,128)(2,1)}), bf16[1376,2048]{1,0:T(8,128)(2,1)}) %all-gather.19.cloned.1.call-update) | async-done | bytes 5636112 | tf_op jit(solution)/shard_map/all_gather | solution.py:48
  325.1 20.8 %convolution_convert_fusion.1 = bf16[1024,2048]{1,0:T(8,128)(2,1)} fusion(bf16[1376,2048]{1,0:T(8,128)(2,1)} %all-gather.19.cloned.1.call-done, f32[1024,1376]{0,1:T(8,128)} %fusion.65, bf16[1024,2048]{1,0:T(8,128)(2,1)} %all-gather.13.cloned.1.call-done, bf16[2048,1376]{0,1:T(8,128)(2,1)} %all-gather.17.cloned.1.call-done), kind=kOutput, calls=%fused_computation.7 | convolution fusion | flops 11553275904 | bytes 25296896 | tf_op jit(solution)/shard_map/dot_general | solution.py:51
  346.6 42.3 %reduce-scatter.4.cloned.1.call-done = bf16[256,2048]{1,0:T(8,128)(2,1)} async-done(((bf16[1024,2048]{1,0:T(8,128)(2,1)}), bf16[256,2048]{1,0:T(8,128)(2,1)}) %reduce-scatter.4.cloned.1.call-update) | async-done | bytes 1048592 | tf_op jit(solution)/shard_map/reduce_scatter | solution.py:50
  388.8 1.8 fusion.13
  393.7 57.2 %all-gather.25.cloned.1.call-done = bf16[2048,768]{1,0:T(8,128)(2,1)} async-done(((bf16[256,768]{1,0:T(8,128)(2,1)}), bf16[2048,768]{1,0:T(8,128)(2,1)}) %all-gather.25.cloned.1.call-update) | async-done | bytes 3145744 | tf_op jit(solution)/shard_map/all_gather | solution.py:37
  450.9 34.7 %all-gather.21.cloned.1.call-done = bf16[1024,2048]{1,0:T(8,128)(2,1)} async-done(((bf16[256,2048]{1,0:T(8,128)(2,1)}), bf16[1024,2048]{1,0:T(8,128)(2,1)}) %all-gather.21.cloned.1.call-update) | async-done | bytes 4194320 | tf_op jit(solution)/shard_map/all_gather | solution.py:33
  485.6 6.6 fusion.33
  492.2 1.6 pad.81
  493.8 2.0 reshape.51
  496.2 2.6 select_convert_fusion
  500.3 1.9 reshape.55
  503.5 2.6 copy.33
  506.2 4.1 add_divide_fusion.1
  510.3 3.6 copy.35
  513.9 4.2 add_divide_fusion
  518.0 3.5 copy.37
  521.6 8.1 fusion.8
  529.7 8.1 slice.234
  537.8 8.1 slice.235
  545.9 8.1 slice.233
  554.1 8.2 slice.237
  562.3 4.4 fusion.55
  566.6 2.8 slice.240
  569.4 2.8 slice.241
  572.2 4.8 slice.239
  577.0 4.8 slice.243
  581.8 3.3 fusion.56
  585.0 3.0 slice.246
  588.1 3.1 slice.247
  591.1 3.1 slice.245
  594.2 3.0 slice.249
  601.7 2.1 fusion.58
  606.9 1.6 slice.257
  610.0 1.7 fusion.59
  644.6 1.6 slice.297
  649.7 2.1 slice.244
  651.8 3.1 slice.301
  656.2 4.8 slice.238
  661.0 2.8 slice.303
  664.5 8.2 slice.305
  672.8 8.4 slice.232
  689.2 2.3 pad.77
  691.5 5.2 pad.78
  696.7 2.8 add.244
  699.5 9.7 pad.80
  709.2 2.7 fusion.28
  712.0 5.7 pad.79
  717.7 14.9 %convolution_convert_fusion.2 = bf16[1024,2048]{1,0:T(8,128)(2,1)} fusion(bf16[768,2048]{1,0:T(8,128)(2,1)} %all-gather.27.cloned.1.call-done, f32[1024,768]{1,0:T(8,128)} %pad.79, f32[1024,768]{1,0:T(8,128)} %pad.80, bf16[1024,2048]{1,0:T(8,128)(2,1)} %all-gather.21.cloned.1.call-done, bf16[2048,768]{1,0:T(8,128)(2,1)} %all-gather.23.cloned.1.call-done), kind=kOutput, calls=%fused_computation.8 | convolution fusion | flops 6454771712 | bytes 20971520 | tf_op jit(solution)/shard_map/dot_general | solution.py:51
  733.5 44.2 %reduce-scatter.6.cloned.1.call-done = bf16[256,2048]{1,0:T(8,128)(2,1)} async-done(((bf16[1024,2048]{1,0:T(8,128)(2,1)}), bf16[256,2048]{1,0:T(8,128)(2,1)}) %reduce-scatter.6.cloned.1.call-update) | async-done | bytes 1048592 | tf_op jit(solution)/shard_map/reduce_scatter | solution.py:50
  777.7 1.6 fusion.17
  779.3 2.6 fusion.19
  783.3 88.0 %all-gather.31.cloned.1.call-done = bf16[2048,1376]{0,1:T(8,128)(2,1)} async-done(((bf16[256,1376]{0,1:T(8,128)(2,1)}), bf16[2048,1376]{0,1:T(8,128)(2,1)}) %all-gather.31.cloned.1.call-update) | async-done | bytes 5636112 | tf_op jit(solution)/shard_map/all_gather | solution.py:37
  871.3 34.1 %all-gather.29.cloned.1.call-done = bf16[1024,2048]{1,0:T(8,128)(2,1)} async-done(((bf16[256,2048]{1,0:T(8,128)(2,1)}), bf16[1024,2048]{1,0:T(8,128)(2,1)}) %all-gather.29.cloned.1.call-update) | async-done | bytes 4194320 | tf_op jit(solution)/shard_map/all_gather | solution.py:33
  905.4 11.1 fusion.66
  916.5 82.5 %all-gather.33.cloned.1.call-done = bf16[2048,1376]{0,1:T(8,128)(2,1)} async-done(((bf16[256,1376]{0,1:T(8,128)(2,1)}), bf16[2048,1376]{0,1:T(8,128)(2,1)}) %all-gather.33.cloned.1.call-update) | async-done | bytes 5636112 | tf_op jit(solution)/shard_map/all_gather | solution.py:38
  999.0 91.7 %all-gather.35.cloned.1.call-done = bf16[1376,2048]{1,0:T(8,128)(2,1)} async-done(((bf16[1376,256]{1,0:T(8,128)(2,1)}), bf16[1376,2048]{1,0:T(8,128)(2,1)}) %all-gather.35.cloned.1.call-update) | async-done | bytes 5636112 | tf_op jit(solution)/shard_map/all_gather | solution.py:48
  1090.7 20.8 %convolution_convert_fusion = bf16[1024,2048]{1,0:T(8,128)(2,1)} fusion(bf16[1376,2048]{1,0:T(8,128)(2,1)} %all-gather.35.cloned.1.call-done, f32[1024,1376]{0,1:T(8,128)} %fusion.66, bf16[1024,2048]{1,0:T(8,128)(2,1)} %all-gather.29.cloned.1.call-done, bf16[2048,1376]{0,1:T(8,128)(2,1)} %all-gather.33.cloned.1.call-done), kind=kOutput, calls=%fused_computation.6 | convolution fusion | flops 11553275904 | bytes 25296896 | tf_op jit(solution)/shard_map/dot_general | solution.py:51
  1111.5 42.9 %reduce-scatter.8.cloned.1.call-done = bf16[256,2048]{1,0:T(8,128)(2,1)} async-done(((bf16[1024,2048]{1,0:T(8,128)(2,1)}), bf16[256,2048]{1,0:T(8,128)(2,1)}) %reduce-scatter.8.cloned.1.call-update) | async-done | bytes 1048592 | tf_op jit(solution)/shard_map/reduce_scatter | solution.py:50
  1154.4 2.7 fusion.20
  (191 shorter events, 67.7 us)
Async XLA Ops:
  6.5 499.6 %copy-start = (bf16[4,192,192]{2,1,0:T(8,128)(2,1)S(1)}, bf16[4,192,192]{2,1,0:T(8,128)(2,1)}, u32[]{:S(2)}) copy-start(bf16[4,192,192]{2,1,0:T(8,128)(2,1)} %param.27) | copy-start | bytes 884740
  6.5 41.4 %all-gather.13.cloned.1.call-start = ((), (), s32[]{:S(2)}) async-start(), calls=%async_computation.3 | async-start | bytes 5242880 | tf_op jit(solution)/shard_map/all_gather | solution.py:33
  10.6 131.0 %all-gather.15.cloned.1.call-start = ((), (), s32[]{:S(2)}) async-start(), calls=%async_computation.4 | async-start | bytes 6340608 | tf_op jit(solution)/shard_map/all_gather | solution.py:37
  11.4 222.0 %all-gather.17.cloned.1.call-start = ((), (), s32[]{:S(2)}) async-start(), calls=%async_computation.5 | async-start | bytes 6340608 | tf_op jit(solution)/shard_map/all_gather | solution.py:38
  12.1 312.9 %all-gather.19.cloned.1.call-start = ((), (), s32[]{:S(2)}) async-start(), calls=%async_computation.6 | async-start | bytes 6340608 | tf_op jit(solution)/shard_map/all_gather | solution.py:48
  12.7 376.1 %reduce-scatter.4.cloned.1.call-start = ((), (), s32[]{:S(2)}) async-start(), calls=%async_computation.7 | async-start | bytes 5242880 | tf_op jit(solution)/shard_map/reduce_scatter | solution.py:50
  345.9 42.9 %copy-start.2 = (bf16[256,2048]{1,0:T(8,128)(2,1)S(1)}, bf16[256,2048]{1,0:T(8,128)(2,1)}, u32[]{:S(2)}) copy-start(bf16[256,2048]{1,0:T(8,128)(2,1)} %param.18) | copy-start | bytes 3145732
  345.9 44.7 %copy-start.25 = (f32[2048]{0:T(1024)S(1)}, f32[2048]{0:T(1024)}, u32[]{:S(2)}) copy-start(f32[2048]{0:T(1024)} %param.23) | copy-start | bytes 24580
  345.9 105.0 %all-gather.25.cloned.1.call-start = ((), (), s32[]{:S(2)}) async-start(), calls=%async_computation.10 | async-start | bytes 3538944 | tf_op jit(solution)/shard_map/all_gather | solution.py:37
  346.5 47.2 %copy-start.28 = (f32[768]{0:T(1024)S(1)}, f32[768]{0:T(1024)}, u32[]{:S(2)}) copy-start(f32[768]{0:T(1024)} %param.29) | copy-start | bytes 9220
  346.5 139.1 %all-gather.21.cloned.1.call-start = ((), (), s32[]{:S(2)}) async-start(), calls=%async_computation.8 | async-start | bytes 5242880 | tf_op jit(solution)/shard_map/all_gather | solution.py:33
  392.0 325.8 %all-gather.23.cloned.1.call-start = ((), (), s32[]{:S(2)}) async-start(), calls=%async_computation.9 | async-start | bytes 3538944 | tf_op jit(solution)/shard_map/all_gather | solution.py:38
  392.7 325.0 %all-gather.27.cloned.1.call-start = ((), (), s32[]{:S(2)}) async-start(), calls=%async_computation.11 | async-start | bytes 3538944 | tf_op jit(solution)/shard_map/all_gather | solution.py:48
  393.4 384.2 %reduce-scatter.6.cloned.1.call-start = ((), (), s32[]{:S(2)}) async-start(), calls=%async_computation.12 | async-start | bytes 5242880 | tf_op jit(solution)/shard_map/reduce_scatter | solution.py:50
  493.8 2.3 copy-start.30
  493.8 2.3 copy-start.31
  510.3 3.6 copy-start.29
  518.0 3.5 copy-start.27
  664.4 18.1 %copy-start.13 = (f32[2,768]{1,0:T(2,128)S(1)}, f32[2,768]{1,0:T(2,128)}, u32[]{:S(2)}) copy-start(f32[2,768]{1,0:T(2,128)} %slice.281) | copy-start | bytes 18436
  664.4 18.1 %copy-start.14 = (f32[2,768]{1,0:T(2,128)S(1)}, f32[2,768]{1,0:T(2,128)}, u32[]{:S(2)}) copy-start(f32[2,768]{1,0:T(2,128)} %slice.282) | copy-start | bytes 18436
  664.5 18.1 %copy-start.15 = (f32[2,768]{1,0:T(2,128)S(1)}, f32[2,768]{1,0:T(2,128)}, u32[]{:S(2)}) copy-start(f32[2,768]{1,0:T(2,128)} %slice.283) | copy-start | bytes 18436
  664.5 18.2 %copy-start.16 = (f32[2,768]{1,0:T(2,128)S(1)}, f32[2,768]{1,0:T(2,128)}, u32[]{:S(2)}) copy-start(f32[2,768]{1,0:T(2,128)} %slice.285) | copy-start | bytes 18436
  664.5 18.2 %copy-start.10 = (f32[4,768]{1,0:T(4,128)S(1)}, f32[4,768]{1,0:T(4,128)}, u32[]{:S(2)}) copy-start(f32[4,768]{1,0:T(4,128)} %get-tuple-element.26) | copy-start | bytes 36868
  664.5 19.0 %copy-start.11 = (f32[3,768]{1,0:T(4,128)S(1)}, f32[3,768]{1,0:T(4,128)}, u32[]{:S(2)}) copy-start(f32[3,768]{1,0:T(4,128)} %slice.274) | copy-start | bytes 27652
  664.5 19.0 %copy-start.12 = (f32[3,768]{1,0:T(4,128)S(1)}, f32[3,768]{1,0:T(4,128)}, u32[]{:S(2)}) copy-start(f32[3,768]{1,0:T(4,128)} %slice.291) | copy-start | bytes 27652
  664.5 19.0 %copy-start.22 = (f32[1,768]{1,0:T(1,128)S(1)}, f32[1,768]{1,0:T(1,128)}, u32[]{:S(2)}) copy-start(f32[1,768]{1,0:T(1,128)} %slice.317) | copy-start | bytes 9220
  664.5 19.1 %copy-start.8 = (f32[7,768]{1,0:T(8,128)S(1)}, f32[7,768]{1,0:T(8,128)}, u32[]{:S(2)}) copy-start(f32[7,768]{1,0:T(8,128)} %slice.268) | copy-start | bytes 64516
  664.5 19.1 %copy-start.9 = (f32[7,768]{1,0:T(8,128)S(1)}, f32[7,768]{1,0:T(8,128)}, u32[]{:S(2)}) copy-start(f32[7,768]{1,0:T(8,128)} %slice.293) | copy-start | bytes 64516
  664.5 19.1 %copy-start.21 = (f32[1,768]{1,0:T(1,128)S(1)}, f32[1,768]{1,0:T(1,128)}, u32[]{:S(2)}) copy-start(f32[1,768]{1,0:T(1,128)} %slice.316) | copy-start | bytes 9220
  664.5 19.2 %copy-start.7 = (f32[15,768]{1,0:T(8,128)S(1)}, f32[15,768]{1,0:T(8,128)}, u32[]{:S(2)}) copy-start(f32[15,768]{1,0:T(8,128)} %slice.295) | copy-start | bytes 138244
  664.5 19.2 %copy-start.20 = (f32[1,768]{1,0:T(1,128)S(1)}, f32[1,768]{1,0:T(1,128)}, u32[]{:S(2)}) copy-start(f32[1,768]{1,0:T(1,128)} %slice.315) | copy-start | bytes 9220
  672.8 11.1 copy-start.6
  672.8 11.1 copy-start.23
  672.8 11.2 copy-start.4
  672.8 11.2 copy-start.5
  672.8 11.3 copy-start.19
  684.1 1.4 copy-start.18
  685.7 2.5 copy-start.24
  709.2 2.7 copy-start.17
  732.6 46.7 %copy-start.26 = (f32[2048]{0:T(1024)S(1)}, f32[2048]{0:T(1024)}, u32[]{:S(2)}) copy-start(f32[2048]{0:T(1024)} %param.32) | copy-start | bytes 24580
  732.7 138.6 %all-gather.31.cloned.1.call-start = ((), (), s32[]{:S(2)}) async-start(), calls=%async_computation.14 | async-start | bytes 6340608 | tf_op jit(solution)/shard_map/all_gather | solution.py:37
  733.4 172.0 %all-gather.29.cloned.1.call-start = ((), (), s32[]{:S(2)}) async-start(), calls=%async_computation.13 | async-start | bytes 5242880 | tf_op jit(solution)/shard_map/all_gather | solution.py:33
  781.9 217.1 %all-gather.33.cloned.1.call-start = ((), (), s32[]{:S(2)}) async-start(), calls=%async_computation.15 | async-start | bytes 6340608 | tf_op jit(solution)/shard_map/all_gather | solution.py:38
  782.7 308.0 %all-gather.35.cloned.1.call-start = ((), (), s32[]{:S(2)}) async-start(), calls=%async_computation.16 | async-start | bytes 6340608 | tf_op jit(solution)/shard_map/all_gather | solution.py:48
  783.3 371.1 %reduce-scatter.8.cloned.1.call-start = ((), (), s32[]{:S(2)}) async-start(), calls=%async_computation.17 | async-start | bytes 5242880 | tf_op jit(solution)/shard_map/reduce_scatter | solution.py:50
  1111.5 42.9 %copy-start.3 = (bf16[256,2048]{1,0:T(8,128)(2,1)S(1)}, bf16[256,2048]{1,0:T(8,128)(2,1)}, u32[]{:S(2)}) copy-start(bf16[256,2048]{1,0:T(8,128)(2,1)} %reduce-scatter.6.cloned.1.call-done) | copy-start | bytes 3145732
  1111.5 45.7 %copy-start.1 = (bf16[4,192,192]{2,1,0:T(8,128)(2,1)S(1)}, bf16[4,192,192]{2,1,0:T(8,128)(2,1)}, u32[]{:S(2)}) copy-start(bf16[4,192,192]{2,1,0:T(8,128)(2,1)} %param.27) | copy-start | bytes 884740
Sparse Core Ops, SparseCore 0:
  10.8 37.1 all-gather.12
  50.0 91.5 all-gather.14
  143.7 89.7 all-gather.16
  235.3 89.7 all-gather.18
  346.0 42.7 reduce-scatter.3
  390.9 60.0 all-gather.24
  452.5 33.1 all-gather.20
  487.8 60.0 all-gather.22
  549.9 61.2 all-gather.26
  732.8 44.8 reduce-scatter.5
  779.7 91.5 all-gather.30
  872.7 32.6 all-gather.28
  907.4 91.5 all-gather.32
  1000.9 89.7 all-gather.34
  1111.6 42.7 reduce-scatter.7
where the time goes:
time: 1180 us; the launch traced here: 1160 us
  waiting for transfers between devices  825 us (70%)
  local copies, waits for them, and re-layouts  178 us (15%)
  matrix products  95.9 us (8%)
  other arithmetic  50.6 us (4%)
  between operations  14.4 us (1%)
    all_gather x3, waiting for transfers between devices, sublayer(): lax.all_gather(first_weight, 'fs', axis=0, tiled=True)  239 us
    all_gather x3, waiting for transfers between devices, sublayer(): full_out = lax.all_gather(out_weight, 'fs', axis=1, tiled=True)  183 us
    all_gather x3, waiting for transfers between devices, sublayer(): lax.all_gather(second_weight, 'fs', axis=0, tiled=True)  164 us
    slice x60, local copies, waits for them, and re-layouts, recurrent(): lax.associative_scan(combine, (decay_rate, drive_in), axis=0)  136 us
    reduce_scatter x3, waiting for transfers between devices, sublayer(): lax.psum_scatter(jnp.dot(picked, full_out, preferred_element_type=jnp.flo...  129 us
    all_gather x3, waiting for transfers between devices, sublayer(): whole = lax.all_gather(normal, 'tp', axis=0, tiled=True)  104 us
    dot_general x3, matrix products, sublayer(): jnp.dot(picked, full_out, preferred_element_type=jnp.float32)  56.6 us
    dot_general x3, matrix products, sublayer(): jnp.dot(columns, pieces[0], preferred_element_type=jnp.float32)  28.5 us
  transfers between devices with their start and end apart: 15, of which 13 were waited for; matrix products, arithmetic and copies ran while one was open for 22% of the time, Pallas kernels for 0%

commit v1 on v0

v1 whole, which is shorter than its diff:
```python
import functools

import jax
import jax.numpy as jnp
from jax import lax
from jax.experimental import pallas as pl
from jax.sharding import PartitionSpec as P


EPS = 1e-06
RECURRENT_WIDTH = 8.0
ROW_TILE = 128


def normed(input_token_rows, norm_scale_vector):
    values = input_token_rows.astype(jnp.float32)
    square = jnp.mean(values * values, axis=-1, keepdims=True)
    return (values * lax.rsqrt(square + EPS) * norm_scale_vector).astype(jnp.bfloat16)


def swap(value, axis, distance):
    size = lax.axis_size(axis)
    return lax.ppermute(value, axis, [(i, i ^ distance) for i in range(size)])


def order_pair(own, other, bit):
    return jnp.where(bit, other, own), jnp.where(bit, own, other)


def gather_rows(rows):
    size = lax.axis_size("tp")
    index = lax.axis_index("tp")
    held = rows[None]
    distance = size // 2
    while distance:
        other = swap(held, "tp", distance)
        low, high = order_pair(held, other, (index // distance) % 2 == 1)
        held = jnp.stack([low, high], axis=1).reshape((2 * held.shape[0],) + rows.shape)
        distance //= 2
    return held.reshape((-1,) + rows.shape[1:])


def half_of(rows, distance, bit):
    cut = rows.reshape((rows.shape[0] // (2 * distance), 2, distance) + rows.shape[1:])
    picked = lax.dynamic_index_in_dim(cut, bit, 1, keepdims=False)
    return picked.reshape((-1,) + rows.shape[1:])


def project_scatter(hidden, weight, row_count):
    size = lax.axis_size("tp")
    index = lax.axis_index("tp")
    blocks = hidden.reshape(size, row_count, hidden.shape[1])

    def product(part):
        flat = part.reshape(-1, part.shape[-1])
        out = jnp.dot(flat, weight, preferred_element_type=jnp.float32).astype(jnp.bfloat16)
        return out.reshape(part.shape[0], row_count, -1)

    bit = index % 2
    sent = swap(product(half_of(blocks, 1, 1 - bit)), "tp", 1)
    kept = product(half_of(blocks, 1, bit)).astype(jnp.float32) + sent.astype(jnp.float32)
    distance = 2
    while distance < size:
        bit = (index // distance) % 2
        cut = kept.reshape((-1, 2) + kept.shape[1:])
        mine = lax.dynamic_index_in_dim(cut, bit, 1, keepdims=False)
        theirs = lax.dynamic_index_in_dim(cut, 1 - bit, 1, keepdims=False)
        arrived = swap(theirs.astype(jnp.bfloat16), "tp", distance)
        kept = mine + arrived.astype(jnp.float32)
        distance *= 2
    return kept.reshape(row_count, -1)


def parity_groups(size):
    return [list(range(0, size, 2)), list(range(1, size, 2))]


def gather_weight(weight, dim):
    own = lax.all_gather(
        weight, "fs", axis=dim, tiled=True, axis_index_groups=parity_groups(lax.axis_size("fs"))
    )
    return own, swap(own, "fs", 1)


def split_features(rows):
    size = lax.axis_size("fs")
    bit = lax.axis_index("fs") % 2
    cut = rows.reshape(rows.shape[0], size // 2, 2, rows.shape[1] // size)
    even, odd = cut[:, :, 0].reshape(rows.shape[0], -1), cut[:, :, 1].reshape(rows.shape[0], -1)
    return order_pair(even, odd, bit == 1)


def join_features(own, other):
    size = lax.axis_size("fs")
    bit = lax.axis_index("fs") % 2
    even, odd = order_pair(own, other, bit == 1)
    shape = (own.shape[0], size // 2, own.shape[1] * 2 // size)
    return jnp.stack([even.reshape(shape), odd.reshape(shape)], axis=2).reshape(own.shape[0], -1)


def recurrence_kernel(
    recur_ref, branch_ref, taps_ref, decay_ref, input_ref, rate_ref, extra_ref, out_ref, *, tile
):
    length, width = recur_ref.shape
    taps = taps_ref.shape[0]

    def shifted(value, steps, fill):
        return jnp.concatenate(
            [jnp.full((steps, width), fill, jnp.float32), value[: tile - steps]], axis=0
        )

    def body(step, carry):
        tail, state = carry
        at = pl.ds(pl.multiple_of(step * tile, tile), tile)
        rows = recur_ref[at, :].astype(jnp.float32)
        longer = jnp.concatenate([tail, rows], axis=0)
        summed = jnp.zeros((tile, width), jnp.float32)
        for j in range(taps):
            start = 8 - (taps - 1) + j
            summed = summed + longer[start : start + tile] * taps_ref[j : j + 1, :]
        conv_out = summed.astype(jnp.bfloat16)
        rate_gate = jax.nn.sigmoid(
            jnp.dot(conv_out, decay_ref[...], preferred_element_type=jnp.float32)
        )
        input_gate = jax.nn.sigmoid(
            jnp.dot(conv_out, input_ref[...], preferred_element_type=jnp.float32)
        )
        log_a = rate_gate * rate_ref[...] + extra_ref[at, :]
        decay = jnp.exp(log_a)
        twice = 2.0 * log_a
        near_zero = -twice * (1.0 + twice * (0.5 + twice * (1.0 / 6.0)))
        left = jnp.where(twice > -0.03, near_zero, 1.0 - decay * decay)
        drive = jnp.sqrt(left) * input_gate * conv_out.astype(jnp.float32)
        steps = 1
        while steps < tile:
            drive = drive + decay * shifted(drive, steps, 0.0)
            decay = decay * shifted(decay, steps, 1.0)
            steps *= 2
        hidden = drive + decay * state
        branch = branch_ref[at, :].astype(jnp.float32)
        inner = 0.7978845608028654 * (branch + 0.044715 * branch * branch * branch)
        gelu = 0.5 * branch * (1.0 + jnp.tanh(inner))
        out_ref[at, :] = (gelu * hidden).astype(jnp.bfloat16)
        return rows[tile - 8 :], hidden[tile - 1 :]

    first = (jnp.zeros((8, width), jnp.float32), jnp.zeros((1, width), jnp.float32))
    lax.fori_loop(0, length // tile, body, first)


def block_diagonal(blocks, group):
    count, size, _ = blocks.shape
    parts = blocks.reshape(count // group, group, size, size)
    eye = jnp.eye(group, dtype=blocks.dtype)
    wide = parts[:, :, :, None, :] * eye[None, :, None, :, None]
    return wide.reshape(count // group, group * size, group * size)


def recurrence(recur, branch, taps, decay_blocks, input_blocks, decay_weight, extra):
    length, channels = recur.shape
    size = decay_blocks.shape[1]
    group = 1
    while (group * size) % 128 and decay_blocks.shape[0] % (2 * group) == 0:
        group *= 2
    width = group * size
    rate = (-RECURRENT_WIDTH * jax.nn.softplus(-decay_weight))[None]
    tile = ROW_TILE if length % ROW_TILE == 0 else length
    column = lambda i: (0, i)
    return pl.pallas_call(
        functools.partial(recurrence_kernel, tile=tile),
        grid=(channels // width,),
        in_specs=[
            pl.BlockSpec((length, width), column),
            pl.BlockSpec((length, width), column),
            pl.BlockSpec((taps.shape[0], width), column),
            pl.BlockSpec((None, width, width), lambda i: (i, 0, 0)),
            pl.BlockSpec((None, width, width), lambda i: (i, 0, 0)),
            pl.BlockSpec((1, width), column),
            pl.BlockSpec((length, 1), lambda i: (0, 0)),
        ],
        out_specs=pl.BlockSpec((length, width), column),
        out_shape=jax.ShapeDtypeStruct((length, channels), jnp.bfloat16),
        cost_estimate=pl.CostEstimate(
            flops=4 * length * channels * width * 4,
            bytes_accessed=6 * length * channels,
            transcendentals=6 * length * channels,
        ),
    )(
        recur,
        branch,
        taps,
        block_diagonal(decay_blocks, group),
        block_diagonal(input_blocks, group),
        rate,
        extra[:, None],
    )


def sublayer(residual, norm_scale_vector, first, second, out, middle):
    rows = gather_rows(jnp.stack(split_features(normed(residual, norm_scale_vector)), axis=1))
    own, other = rows[:, 0], rows[:, 1]

    def project(pair):
        return jnp.dot(own, pair[0], preferred_element_type=jnp.float32) + jnp.dot(
            other, pair[1], preferred_element_type=jnp.float32
        )

    hidden = middle(project(first), project(second))
    count = residual.shape[0]
    return join_features(
        project_scatter(hidden, out[0], count), project_scatter(hidden, out[1], count)
    )


def shards(
    tokens,
    first_block_norm_scale,
    first_block_gate_matrix,
    first_block_up_matrix,
    first_block_down_matrix,
    mixer_norm_scale,
    recurrent_input_matrix,
    output_gate_projection,
    convolution_kernel,
    decay_gate_blocks,
    input_gate_blocks,
    channel_decay_weight,
    position_decay_extra,
    mixer_output_matrix,
    second_block_norm_scale,
    second_block_gate_matrix,
    second_block_up_matrix,
    second_block_down_matrix,
):
    def feed_middle(gate_pre, up_pre):
        return (jax.nn.silu(gate_pre) * up_pre).astype(jnp.bfloat16)

    def mixer_middle(recur_pre, branch_pre):
        return recurrence(
            recur_pre.astype(jnp.bfloat16),
            branch_pre.astype(jnp.bfloat16),
            convolution_kernel,
            decay_gate_blocks,
            input_gate_blocks,
            channel_decay_weight,
            position_decay_extra,
        )

    first_weights = [
        gather_weight(first_block_gate_matrix, 0),
        gather_weight(first_block_up_matrix, 0),
        gather_weight(first_block_down_matrix, 1),
    ]
    mixer_weights = [
        gather_weight(recurrent_input_matrix, 0),
        gather_weight(output_gate_projection, 0),
        gather_weight(mixer_output_matrix, 1),
    ]
    second_weights = [
        gather_weight(second_block_gate_matrix, 0),
        gather_weight(second_block_up_matrix, 0),
        gather_weight(second_block_down_matrix, 1),
    ]
    residual = tokens
    change = sublayer(residual, first_block_norm_scale, *first_weights, feed_middle)
    residual = (residual.astype(jnp.float32) + 0.5 * change).astype(jnp.bfloat16)
    change = sublayer(residual, mixer_norm_scale, *mixer_weights, mixer_middle)
    residual = (residual.astype(jnp.float32) + change).astype(jnp.bfloat16)
    change = sublayer(residual, second_block_norm_scale, *second_weights, feed_middle)
    return (residual.astype(jnp.float32) + 0.5 * change).astype(jnp.bfloat16)


def solution(mesh):
    in_specs = (
        P(("fs", "tp"), None),
        P(),
        P("fs", "tp"),
        P("fs", "tp"),
        P("tp", "fs"),
        P(),
        P("fs", "tp"),
        P("fs", "tp"),
        P(None, "tp"),
        P("tp", None, None),
        P("tp", None, None),
        P("tp"),
        P("fs"),
        P("tp", "fs"),
        P(),
        P("fs", "tp"),
        P("fs", "tp"),
        P("tp", "fs"),
    )
    out_specs = P(("fs", "tp"), None)

    return jax.shard_map(shards, mesh=mesh, in_specs=in_specs, out_specs=out_specs, check_vma=False)
```

time: 1180 us -> 759 us (0.64)
  waiting for transfers between devices: 825 us -> 450 us
  local copies, waits for them, and re-layouts: 178 us -> 102 us
  starting transfers between devices: 0.73 us -> 25.4 us
  Pallas kernels: 0 us -> 15.9 us
  other arithmetic: 50.6 us -> 37.2 us
    all_gather x12 -> x9, waiting for transfers between devices: 690 us -> 131 us  [gather_weight(): lax.all_gather(weight, 'fs', axis=dim, tiled=True, axis_index_groups=pari...]
    ppermute x0 -> x27, waiting for transfers between devices: none -> 316 us  [swap(): return lax.ppermute(value, axis, [(i, i ^ distance) for i in range(size)])]
    slice x60 -> x0, local copies, waits for them, and re-layouts: 136 us -> none  [recurrent(): lax.associative_scan(combine, (decay_rate, drive_in), axis=0)]
    reduce_scatter x3 -> x0, waiting for transfers between devices: 129 us -> none  [sublayer(): lax.psum_scatter(jnp.dot(picked, full_out, preferred_element_type=jnp.flo...]
    another operation x0 -> x5, local copies, waits for them, and re-layouts: none -> 32.6 us  [the longest x3 19.6 us: gather_rows(): jnp.stack([low, high], axis=1).reshape((2 * held.shape[0],) + rows.shape)]
    unnamed x64 -> x65, local copies, waits for them, and re-layouts: 0.13 us -> 31.6 us
    ppermute x0 -> x27, starting transfers between devices: none -> 25.1 us  [swap(): return lax.ppermute(value, axis, [(i, i ^ distance) for i in range(size)])]
    pad x18 -> x0, local copies, waits for them, and re-layouts: 23.4 us -> none  [recurrent(): lax.associative_scan(combine, (decay_rate, drive_in), axis=0)]
  transfers between devices with their start and end apart: 15 -> 36, of which waited for: 13 -> 20; matrix products, arithmetic and copies ran while one was open for 22% -> 31% of each run, Pallas kernels for 0% -> 2%
where the time goes in v1:
time: 759 us; the launch traced here: 747 us
  waiting for transfers between devices  450 us (59%)
  matrix products  103 us (14%)
  local copies, waits for them, and re-layouts  102 us (13%)
  other arithmetic  37.2 us (5%)
  starting transfers between devices  25.4 us (3%)
  Pallas kernels  15.9 us (2%)
  between operations  14.5 us (2%)
    ppermute x27, waiting for transfers between devices, swap(): return lax.ppermute(value, axis, [(i, i ^ distance) for i in range(size)])  316 us
    all_gather x9, waiting for transfers between devices, gather_weight(): lax.all_gather(weight, 'fs', axis=dim, tiled=True, axis_index_groups=pari...  131 us
    dot_general x12, matrix products, product(): jnp.dot(flat, weight, preferred_element_type=jnp.float32)  42.6 us
    dot_general x6, matrix products, project(): jnp.dot(other, pair[1], preferred_element_type=jnp.float32)  37.9 us
    unnamed x65, local copies, waits for them, and re-layouts  31.6 us
    ppermute x27, starting transfers between devices, swap(): return lax.ppermute(value, axis, [(i, i ^ distance) for i in range(size)])  25.1 us
    dot_general x6, matrix products, project(): jnp.dot(own, pair[0], preferred_element_type=jnp.float32)  22 us
    another operation x3, local copies, waits for them, and re-layouts, gather_rows(): jnp.stack([low, high], axis=1).reshape((2 * held.shape[0],) + rows.shape)  19.6 us
  transfers between devices with their start and end apart: 36, of which 20 were waited for; matrix products, arithmetic and copies ran while one was open for 31% of the time, Pallas kernels for 2%

profile of v1, /device:TPU:0, one launch (start us, length us, event | category | flops | bytes accessed | tf_op | source)
XLA Modules:
  0.0 747.5 jit_solution(9432493132744661243)
XLA Ops:
  11.0 3.0 collective-permute-start
  14.2 23.2 %collective-permute-done = bf16[1,256,2,1024]{1,3,2,0:T(8,128)(2,1)} collective-permute-done((bf16[1,256,2,1024]{1,3,2,0:T(8,128)(2,1)S(1)}, bf16[1,256,2,1024]{1,3,2,0:T(8,128)(2,1)}, u32[]{:S(2)}, u32[]{:S(2)}) %collective-permute-start) | collective-permute-done | bytes 1048608 | tf_op jit(solution)/shard_map/ppermute | solution.py:23
  40.2 29.5 %all-gather.10.cloned.1.call-done = bf16[1024,1376]{0,1:T(8,128)(2,1)} async-done(((bf16[256,1376]{0,1:T(8,128)(2,1)}), bf16[1024,1376]{0,1:T(8,128)(2,1)}) %all-gather.10.cloned.1.call-update) | async-done | bytes 2818064 | tf_op jit(solution)/shard_map/all_gather | solution.py:79
  71.2 56.3 %all-gather.12.cloned.1.call-done = bf16[1024,1376]{0,1:T(8,128)(2,1)} async-done(((bf16[256,1376]{0,1:T(8,128)(2,1)}), bf16[1024,1376]{0,1:T(8,128)(2,1)}) %all-gather.12.cloned.1.call-update) | async-done | bytes 2818064 | tf_op jit(solution)/shard_map/all_gather | solution.py:79
  129.1 1.9 select_bitcast_fusion.5
  131.0 2.4 pad_maximum_fusion
  133.4 6.6 copy.40
  139.9 45.4 %all-gather.14.cloned.1.call-done = bf16[1376,1024]{1,0:T(8,128)(2,1)} async-done(((bf16[1376,256]{1,0:T(8,128)(2,1)}), bf16[1376,1024]{1,0:T(8,128)(2,1)}) %all-gather.14.cloned.1.call-update) | async-done | bytes 2818064 | tf_op jit(solution)/shard_map/all_gather | solution.py:79
  186.8 4.9 fusion.13
  191.7 3.1 fusion.12
  194.9 6.8 fusion.14
  201.8 8.5 %multiply_convert_fusion.1 = bf16[1024,1376]{0,1:T(8,128)(2,1)} fusion(f32[1024,1376]{0,1:T(8,128)S(1)} %fusion.12, f32[1024,1376]{0,1:T(8,128)S(1)} %fusion.13, f32[1024,1376]{0,1:T(8,128)} %fusion.14, bf16[1024,1376]{0,1:T(8,128)(2,1)} %collective-permute-done.3, bf16[1024,2,1024]{2,0,1:T(8,128)(2,1)S(1)} %bitcast.197), kind=kOutput, calls=%fused_computation.1 | convolution fusion | flops 2896953344 | bytes 24641536 | tf_op jit(solution)/shard_map/dot_general | solution.py:203
  210.3 6.5 reshape_reshape.25
  216.8 7.1 constant_dynamic-slice_fusion.4
  224.0 6.7 copy.62
  230.7 5.1 convolution_convert_fusion.8
  235.8 17.6 %collective-permute-done.4 = bf16[1376,1024]{1,0:T(8,128)(2,1)} collective-permute-done((bf16[1376,1024]{1,0:T(8,128)(2,1)}, bf16[1376,1024]{1,0:T(8,128)(2,1)}, u32[]{:S(2)}, u32[]{:S(2)}) %collective-permute-start.4) | collective-permute-done | bytes 2818080 | tf_op jit(solution)/shard_map/ppermute | solution.py:23
  253.4 5.0 convolution_convert_fusion.10
  258.4 5.6 copy.61
  264.0 4.2 convolution_convert_fusion.9
  268.2 3.7 convolution_convert_fusion.11
  277.6 11.0 %collective-permute-done.8 = bf16[1,256,1024]{2,1,0:T(8,128)(2,1)} collective-permute-done((bf16[1,256,1024]{2,1,0:T(8,128)(2,1)S(1)}, bf16[1,256,1024]{2,1,0:T(8,128)(2,1)}, u32[]{:S(2)}, u32[]{:S(2)}) %collective-permute-start.8) | collective-permute-done | bytes 524320 | tf_op jit(solution)/shard_map/ppermute | solution.py:23
  288.6 10.8 %collective-permute-done.6 = bf16[1,256,1024]{2,1,0:T(8,128)(2,1)} collective-permute-done((bf16[1,256,1024]{2,1,0:T(8,128)(2,1)S(1)}, bf16[1,256,1024]{2,1,0:T(8,128)(2,1)}, u32[]{:S(2)}, u32[]{:S(2)}) %collective-permute-start.6) | collective-permute-done | bytes 524320 | tf_op jit(solution)/shard_map/ppermute | solution.py:23
  299.4 2.8 fusion.23
  308.4 23.0 %collective-permute-done.9 = bf16[1,256,2,1024]{1,3,2,0:T(8,128)(2,1)S(1)} collective-permute-done((bf16[1,256,2,1024]{1,3,2,0:T(8,128)(2,1)S(1)}, bf16[1,256,2,1024]{1,3,2,0:T(8,128)(2,1)S(1)}, u32[]{:S(2)}, u32[]{:S(2)}) %collective-permute-start.9) | collective-permute-done | bytes 1048608 | tf_op jit(solution)/shard_map/ppermute | solution.py:23
  336.2 3.4 mul.148
  339.6 2.3 mul.154
  341.9 3.1 mul.155
  347.9 2.5 broadcast_multiply_fusion
  354.2 2.4 pad_maximum_fusion.1
  356.6 6.4 copy.45
  363.0 7.6 %collective-permute-done.12 = bf16[1024,768]{1,0:T(8,128)(2,1)} collective-permute-done((bf16[1024,768]{1,0:T(8,128)(2,1)}, bf16[1024,768]{1,0:T(8,128)(2,1)}, u32[]{:S(2)}, u32[]{:S(2)}) %collective-permute-start.12) | collective-permute-done | bytes 1572896 | tf_op jit(solution)/shard_map/ppermute | solution.py:23
  370.6 4.0 fusion.17
  374.6 3.0 add_convert_fusion.branch_ref
  377.6 26.7 %collective-permute-done.11 = bf16[1024,768]{1,0:T(8,128)(2,1)} collective-permute-done((bf16[1024,768]{1,0:T(8,128)(2,1)}, bf16[1024,768]{1,0:T(8,128)(2,1)}, u32[]{:S(2)}, u32[]{:S(2)}) %collective-permute-start.11) | collective-permute-done | bytes 1572896 | tf_op jit(solution)/shard_map/ppermute | solution.py:23
  404.3 3.2 fusion.18
  407.6 2.9 add_convert_fusion.1.recur_ref
  410.5 15.9 %shard_map.172 = bf16[1024,768]{1,0:T(8,128)(2,1)} custom-call(bf16[1024,768]{1,0:T(8,128)(2,1)} %add_convert_fusion.1.recur_ref, bf16[1024,768]{1,0:T(8,128)(2,1)} %add_convert_fusion.branch_ref, f32[4,768]{1,0:T(4,128)} %taps_ref.1, bf16[2,384,384]{2,1,0:T(8,128)(2,1)} %get-tuple-element.40.decay_ref, bf16[2,384,384]{2,1,0:T(8,128)(2,1)} %get-tuple-element.39.input_ref, ...), custom_call_target="tpu_custom_call" | custom-call | flops 4831838208 | bytes 4718592 | tf_op jit(solution)/shard_map/pallas_call | solution.py:168
  429.4 8.3 %collective-permute-done.13 = bf16[768,1024]{1,0:T(8,128)(2,1)} collective-permute-done((bf16[768,1024]{1,0:T(8,128)(2,1)}, bf16[768,1024]{1,0:T(8,128)(2,1)}, u32[]{:S(2)}, u32[]{:S(2)}) %collective-permute-start.13) | collective-permute-done | bytes 1572896 | tf_op jit(solution)/shard_map/ppermute | solution.py:23
  437.6 2.4 convolution_convert_fusion.2
  441.1 2.4 convolution_convert_fusion.3
  449.4 10.5 %collective-permute-done.17 = bf16[1,256,1024]{2,1,0:T(8,128)(2,1)} collective-permute-done((bf16[1,256,1024]{2,1,0:T(8,128)(2,1)}, bf16[1,256,1024]{2,1,0:T(8,128)(2,1)}, u32[]{:S(2)}, u32[]{:S(2)}) %collective-permute-start.17) | collective-permute-done | bytes 524320 | tf_op jit(solution)/shard_map/ppermute | solution.py:23
  459.9 10.8 %collective-permute-done.15 = bf16[1,256,1024]{2,1,0:T(8,128)(2,1)} collective-permute-done((bf16[1,256,1024]{2,1,0:T(8,128)(2,1)}, bf16[1,256,1024]{2,1,0:T(8,128)(2,1)}, u32[]{:S(2)}, u32[]{:S(2)}) %collective-permute-start.15) | collective-permute-done | bytes 524320 | tf_op jit(solution)/shard_map/ppermute | solution.py:23
  470.7 3.2 fusion.25
  481.6 23.0 %collective-permute-done.18 = bf16[1,256,2,1024]{1,3,2,0:T(8,128)(2,1)S(1)} collective-permute-done((bf16[1,256,2,1024]{1,3,2,0:T(8,128)(2,1)S(1)}, bf16[1,256,2,1024]{1,3,2,0:T(8,128)(2,1)S(1)}, u32[]{:S(2)}, u32[]{:S(2)}) %collective-permute-start.18) | collective-permute-done | bytes 1048608 | tf_op jit(solution)/shard_map/ppermute | solution.py:23
  512.6 2.4 pad_maximum_fusion.2
  515.0 6.6 copy.49
  521.6 4.9 fusion.20
  526.6 3.1 fusion.19
  529.7 40.7 %collective-permute-done.20 = bf16[1024,1376]{0,1:T(8,128)(2,1)} collective-permute-done((bf16[1024,1376]{0,1:T(8,128)(2,1)}, bf16[1024,1376]{0,1:T(8,128)(2,1)}, u32[]{:S(2)}, u32[]{:S(2)}) %collective-permute-start.20) | collective-permute-done | bytes 2818080 | tf_op jit(solution)/shard_map/ppermute | solution.py:23
  570.5 6.8 fusion.21
  577.3 53.6 %collective-permute-done.21 = bf16[1024,1376]{0,1:T(8,128)(2,1)} collective-permute-done((bf16[1024,1376]{0,1:T(8,128)(2,1)}, bf16[1024,1376]{0,1:T(8,128)(2,1)}, u32[]{:S(2)}, u32[]{:S(2)}) %collective-permute-start.21) | collective-permute-done | bytes 2818080 | tf_op jit(solution)/shard_map/ppermute | solution.py:23
  630.9 8.6 %multiply_convert_fusion = bf16[1024,1376]{0,1:T(8,128)(2,1)} fusion(f32[1024,1376]{0,1:T(8,128)S(1)} %fusion.19, f32[1024,1376]{0,1:T(8,128)S(1)} %fusion.20, f32[1024,1376]{0,1:T(8,128)} %fusion.21, bf16[1024,1376]{0,1:T(8,128)(2,1)} %collective-permute-done.21, bf16[1024,2,1024]{2,0,1:T(8,128)(2,1)S(1)} %bitcast.205), kind=kOutput, calls=%fused_computation | convolution fusion | flops 2896953344 | bytes 24641536 | tf_op jit(solution)/shard_map/dot_general | solution.py:203
  639.4 6.5 reshape_reshape.60
  645.9 7.0 constant_dynamic-slice_fusion
  652.9 6.9 copy.64
  659.9 5.1 convolution_convert_fusion.4
  664.9 25.9 %collective-permute-done.22 = bf16[1376,1024]{1,0:T(8,128)(2,1)} collective-permute-done((bf16[1376,1024]{1,0:T(8,128)(2,1)}, bf16[1376,1024]{1,0:T(8,128)(2,1)}, u32[]{:S(2)}, u32[]{:S(2)}) %collective-permute-start.22) | collective-permute-done | bytes 2818080 | tf_op jit(solution)/shard_map/ppermute | solution.py:23
  690.8 5.0 convolution_convert_fusion.6
  695.8 5.6 copy.63
  701.4 4.1 convolution_convert_fusion.5
  705.6 3.6 convolution_convert_fusion.7
  713.6 12.2 %collective-permute-done.26 = bf16[1,256,1024]{2,1,0:T(8,128)(2,1)S(1)} collective-permute-done((bf16[1,256,1024]{2,1,0:T(8,128)(2,1)S(1)}, bf16[1,256,1024]{2,1,0:T(8,128)(2,1)S(1)}, u32[]{:S(2)}, u32[]{:S(2)}) %collective-permute-start.26) | collective-permute-done | bytes 524320 | tf_op jit(solution)/shard_map/ppermute | solution.py:23
  725.8 10.8 %collective-permute-done.24 = bf16[1,256,1024]{2,1,0:T(8,128)(2,1)S(1)} collective-permute-done((bf16[1,256,1024]{2,1,0:T(8,128)(2,1)S(1)}, bf16[1,256,1024]{2,1,0:T(8,128)(2,1)S(1)}, u32[]{:S(2)}, u32[]{:S(2)}) %collective-permute-start.24) | collective-permute-done | bytes 524320 | tf_op jit(solution)/shard_map/ppermute | solution.py:23
  (179 shorter events, 68.9 us)
Async XLA Ops:
  6.5 2.9 copy-start.16
  6.5 63.2 %all-gather.10.cloned.1.call-start = ((), (), s32[]{:S(2)}) async-start(), calls=%async_computation | async-start | bytes 3522560 | tf_op jit(solution)/shard_map/all_gather | solution.py:79
  7.3 120.2 %all-gather.12.cloned.1.call-start = ((), (), s32[]{:S(2)}) async-start(), calls=%async_computation.1 | async-start | bytes 3522560 | tf_op jit(solution)/shard_map/all_gather | solution.py:79
  8.0 2.3 copy-start.18
  8.0 177.3 %all-gather.14.cloned.1.call-start = ((), (), s32[]{:S(2)}) async-start(), calls=%async_computation.2 | async-start | bytes 3522560 | tf_op jit(solution)/shard_map/all_gather | solution.py:79
  8.8 324.3 %all-gather.18.cloned.1.call-start = ((), (), s32[]{:S(2)}) async-start(), calls=%async_computation.4 | async-start | bytes 1966080 | tf_op jit(solution)/shard_map/all_gather | solution.py:79
  9.3 341.0 %all-gather.16.cloned.1.call-start = ((), (), s32[]{:S(2)}) async-start(), calls=%async_computation.3 | async-start | bytes 1966080 | tf_op jit(solution)/shard_map/all_gather | solution.py:79
  9.9 1.0 copy-start
  11.0 26.3 %collective-permute-start = (bf16[1,256,2,1024]{1,3,2,0:T(8,128)(2,1)S(1)}, bf16[1,256,2,1024]{1,3,2,0:T(8,128)(2,1)}, u32[]{:S(2)}, u32[]{:S(2)}) collective-permute-start(bf16[1,256,2,1024]{1,3,2,0:T(8,128)(2,1)S(1)} %maximum_bitcast_fusion.3), channel_id=1, source_target_pairs={{0,2},{1,3},{2,0},{3,1},{4,6},{5,7},{6,4},{7,5},{8,10},{9,11},{10,... | collective-permute-start | bytes 3145736 | tf_op jit(solution)/shard_map/ppermute | solution.py:23
  14.1 336.5 %all-gather.20.cloned.1.call-start = ((), (), s32[]{:S(2)}) async-start(), calls=%async_computation.5 | async-start | bytes 1966080 | tf_op jit(solution)/shard_map/all_gather | solution.py:79
  40.2 88.9 %collective-permute-start.1 = (bf16[2,256,2,1024]{1,3,2,0:T(8,128)(2,1)}, bf16[2,256,2,1024]{1,3,2,0:T(8,128)(2,1)}, u32[]{:S(2)}, u32[]{:S(2)}) collective-permute-start(bf16[2,256,2,1024]{1,3,2,0:T(8,128)(2,1)} %maximum_bitcast_fusion), channel_id=1, source_target_pairs={{0,1},{1,0},{2,3},{3,2},{4,5},{5,4},{6,7},{7,6},{8,9},{9,8},{10,11... | collective-permute-start | bytes 6291464 | tf_op jit(solution)/shard_map/ppermute | solution.py:23
  69.7 125.2 %collective-permute-start.2 = (bf16[1024,1376]{0,1:T(8,128)(2,1)}, bf16[1024,1376]{0,1:T(8,128)(2,1)}, u32[]{:S(2)}, u32[]{:S(2)}) collective-permute-start(bf16[1024,1376]{0,1:T(8,128)(2,1)} %all-gather.10.cloned.1.call-done), channel_id=1, source_target_pairs={{0,4},{4,0},{8,12},{12,8},{16,20},{20,16},{24,28},{28,24},{1,5},{5... | collective-permute-start | bytes 8454152 | tf_op jit(solution)/shard_map/ppermute | solution.py:23
  127.5 74.2 %collective-permute-start.3 = (bf16[1024,1376]{0,1:T(8,128)(2,1)}, bf16[1024,1376]{0,1:T(8,128)(2,1)}, u32[]{:S(2)}, u32[]{:S(2)}) collective-permute-start(bf16[1024,1376]{0,1:T(8,128)(2,1)} %all-gather.12.cloned.1.call-done), channel_id=1, source_target_pairs={{0,4},{4,0},{8,12},{12,8},{16,20},{20,16},{24,28},{28,24},{1,5},{5... | collective-permute-start | bytes 8454152 | tf_op jit(solution)/shard_map/ppermute | solution.py:23
  129.0 377.2 %all-gather.22.cloned.1.call-start = ((), (), s32[]{:S(2)}) async-start(), calls=%async_computation.6 | async-start | bytes 3522560 | tf_op jit(solution)/shard_map/all_gather | solution.py:79
  133.4 53.5 %copy-start.25 = (bf16[1024,1376]{0,1:T(8,128)(2,1)S(1)}, bf16[1024,1376]{0,1:T(8,128)(2,1)}, u32[]{:S(2)}) copy-start(bf16[1024,1376]{0,1:T(8,128)(2,1)} %all-gather.10.cloned.1.call-done) | copy-start | bytes 8454148
  185.3 68.0 %collective-permute-start.4 = (bf16[1376,1024]{1,0:T(8,128)(2,1)}, bf16[1376,1024]{1,0:T(8,128)(2,1)}, u32[]{:S(2)}, u32[]{:S(2)}) collective-permute-start(bf16[1376,1024]{1,0:T(8,128)(2,1)} %all-gather.14.cloned.1.call-done), channel_id=1, source_target_pairs={{0,4},{4,0},{8,12},{12,8},{16,20},{20,16},{24,28},{28,24},{1,5},{5... | collective-permute-start | bytes 8454152 | tf_op jit(solution)/shard_map/ppermute | solution.py:23
  186.8 4.9 copy-start.8
  186.8 4.9 copy-start.26
  230.7 5.1 copy-start.12
  235.8 22.6 %copy-start.3 = (bf16[2,1,1,256,1376]{3,1,0,4,2:T(2,128)(2,1)S(1)}, bf16[2,1,1,256,1376]{3,1,0,4,2:T(2,128)(2,1)}, u32[]{:S(2)}) copy-start(bf16[2,1,1,256,1376]{3,1,0,4,2:T(2,128)(2,1)} %get-tuple-element.24) | copy-start | bytes 4227076
  235.8 36.1 %collective-permute-start.7 = (bf16[2,256,1024]{2,1,0:T(8,128)(2,1)}, bf16[2,256,1024]{2,1,0:T(8,128)(2,1)}, u32[]{:S(2)}, u32[]{:S(2)}) collective-permute-start(bf16[2,256,1024]{2,1,0:T(8,128)(2,1)} %bitcast.17), channel_id=1, source_target_pairs={{0,1},{1,0},{2,3},{3,2},{4,5},{5,4},{6,7},{7,6},{8,9},{9,8},{10,11... | collective-permute-start | bytes 3145736 | tf_op jit(solution)/shard_map/ppermute | solution.py:23
  264.0 11.4 %collective-permute-start.5 = (bf16[2,256,1024]{2,1,0:T(8,128)(2,1)}, bf16[2,256,1024]{2,1,0:T(8,128)(2,1)S(1)}, u32[]{:S(2)}, u32[]{:S(2)}) collective-permute-start(bf16[2,256,1024]{2,1,0:T(8,128)(2,1)} %bitcast.237), channel_id=1, source_target_pairs={{0,1},{1,0},{2,3},{3,2},{4,5},{5,4},{6,7},{7,6},{8,9},{9,8},{10,11... | collective-permute-start | bytes 3145736 | tf_op jit(solution)/shard_map/ppermute | solution.py:23
  264.0 4.2 copy-start.14
  273.6 15.0 %collective-permute-start.8 = (bf16[1,256,1024]{2,1,0:T(8,128)(2,1)S(1)}, bf16[1,256,1024]{2,1,0:T(8,128)(2,1)}, u32[]{:S(2)}, u32[]{:S(2)}) collective-permute-start(bf16[1,256,1024]{2,1,0:T(8,128)(2,1)S(1)} %dynamic-slice_convert_fusion.4), channel_id=1, source_target_pairs={{0,2},{1,3},{2,0},{3,1},{4,6},{5,7},{6,4},{7,5},{8,10},{9,11},{10,... | collective-permute-start | bytes 1572872 | tf_op jit(solution)/shard_map/ppermute | solution.py:23
  275.8 1.3 copy-start.6
  277.2 22.2 %collective-permute-start.6 = (bf16[1,256,1024]{2,1,0:T(8,128)(2,1)S(1)}, bf16[1,256,1024]{2,1,0:T(8,128)(2,1)}, u32[]{:S(2)}, u32[]{:S(2)}) collective-permute-start(bf16[1,256,1024]{2,1,0:T(8,128)(2,1)S(1)} %dynamic-slice_convert_fusion.5), channel_id=1, source_target_pairs={{0,2},{1,3},{2,0},{3,1},{4,6},{5,7},{6,4},{7,5},{8,10},{9,11},{10,... | collective-permute-start | bytes 1572872 | tf_op jit(solution)/shard_map/ppermute | solution.py:23
  277.6 230.4 %all-gather.24.cloned.1.call-start = ((), (), s32[]{:S(2)}) async-start(), calls=%async_computation.7 | async-start | bytes 3522560 | tf_op jit(solution)/shard_map/all_gather | solution.py:79
  304.1 1.3 copy-start.1
  306.6 24.8 %collective-permute-start.9 = (bf16[1,256,2,1024]{1,3,2,0:T(8,128)(2,1)S(1)}, bf16[1,256,2,1024]{1,3,2,0:T(8,128)(2,1)S(1)}, u32[]{:S(2)}, u32[]{:S(2)}) collective-permute-start(bf16[1,256,2,1024]{1,3,2,0:T(8,128)(2,1)S(1)} %maximum_bitcast_fusion.4), channel_id=1, source_target_pairs={{0,2},{1,3},{2,0},{3,1},{4,6},{5,7},{6,4},{7,5},{8,10},{9,11},{10,... | collective-permute-start | bytes 3145736 | tf_op jit(solution)/shard_map/ppermute | solution.py:23
  331.6 3.3 copy-start.17
  333.1 19.3 %collective-permute-start.10 = (bf16[2,256,2,1024]{1,3,2,0:T(8,128)(2,1)}, bf16[2,256,2,1024]{1,3,2,0:T(8,128)(2,1)}, u32[]{:S(2)}, u32[]{:S(2)}) collective-permute-start(bf16[2,256,2,1024]{1,3,2,0:T(8,128)(2,1)} %maximum_bitcast_fusion.1), channel_id=1, source_target_pairs={{0,1},{1,0},{2,3},{3,2},{4,5},{5,4},{6,7},{7,6},{8,9},{9,8},{10,11... | collective-permute-start | bytes 6291464 | tf_op jit(solution)/shard_map/ppermute | solution.py:23
  333.1 37.6 %collective-permute-start.12 = (bf16[1024,768]{1,0:T(8,128)(2,1)}, bf16[1024,768]{1,0:T(8,128)(2,1)}, u32[]{:S(2)}, u32[]{:S(2)}) collective-permute-start(bf16[1024,768]{1,0:T(8,128)(2,1)} %all-gather.18.cloned.1.call-done), channel_id=1, source_target_pairs={{0,4},{4,0},{8,12},{12,8},{16,20},{20,16},{24,28},{28,24},{1,5},{5... | collective-permute-start | bytes 4718600 | tf_op jit(solution)/shard_map/ppermute | solution.py:23
  334.8 173.4 %all-gather.26.cloned.1.call-start = ((), (), s32[]{:S(2)}) async-start(), calls=%async_computation.8 | async-start | bytes 3522560 | tf_op jit(solution)/shard_map/all_gather | solution.py:79
  339.6 6.6 copy-start.21
  339.6 7.6 %copy-start.22 = (f32[768]{0:T(1024)S(1)}, f32[768]{0:T(1024)}, u32[]{:S(2)}) copy-start(f32[768]{0:T(1024)} %param.29) | copy-start | bytes 9220
  350.3 54.0 %collective-permute-start.11 = (bf16[1024,768]{1,0:T(8,128)(2,1)}, bf16[1024,768]{1,0:T(8,128)(2,1)}, u32[]{:S(2)}, u32[]{:S(2)}) collective-permute-start(bf16[1024,768]{1,0:T(8,128)(2,1)} %all-gather.16.cloned.1.call-done), channel_id=1, source_target_pairs={{0,4},{4,0},{8,12},{12,8},{16,20},{20,16},{24,28},{28,24},{1,5},{5... | collective-permute-start | bytes 4718600 | tf_op jit(solution)/shard_map/ppermute | solution.py:23
  350.6 87.0 %collective-permute-start.13 = (bf16[768,1024]{1,0:T(8,128)(2,1)}, bf16[768,1024]{1,0:T(8,128)(2,1)}, u32[]{:S(2)}, u32[]{:S(2)}) collective-permute-start(bf16[768,1024]{1,0:T(8,128)(2,1)} %all-gather.20.cloned.1.call-done), channel_id=1, source_target_pairs={{0,4},{4,0},{8,12},{12,8},{16,20},{20,16},{24,28},{28,24},{1,5},{5... | collective-permute-start | bytes 4718600 | tf_op jit(solution)/shard_map/ppermute | solution.py:23
  370.6 4.0 copy-start.9
  370.6 4.0 copy-start.27
  377.6 29.9 %copy-start.28 = (bf16[1024,768]{1,0:T(8,128)(2,1)S(1)}, bf16[1024,768]{1,0:T(8,128)(2,1)}, u32[]{:S(2)}) copy-start(bf16[1024,768]{1,0:T(8,128)(2,1)} %all-gather.16.cloned.1.call-done) | copy-start | bytes 4718596
  426.4 1.9 copy-start.29
  429.3 14.2 %collective-permute-start.16 = (bf16[2,256,1024]{2,1,0:T(8,128)(2,1)S(1)}, bf16[2,256,1024]{2,1,0:T(8,128)(2,1)S(1)}, u32[]{:S(2)}, u32[]{:S(2)}) collective-permute-start(bf16[2,256,1024]{2,1,0:T(8,128)(2,1)S(1)} %bitcast.240), channel_id=1, source_target_pairs={{0,1},{1,0},{2,3},{3,2},{4,5},{5,4},{6,7},{7,6},{8,9},{9,8},{10,11... | collective-permute-start | bytes 3145736 | tf_op jit(solution)/shard_map/ppermute | solution.py:23
  440.0 6.5 collective-permute-start.14
  444.8 15.1 %collective-permute-start.17 = (bf16[1,256,1024]{2,1,0:T(8,128)(2,1)}, bf16[1,256,1024]{2,1,0:T(8,128)(2,1)}, u32[]{:S(2)}, u32[]{:S(2)}) collective-permute-start(bf16[1,256,1024]{2,1,0:T(8,128)(2,1)} %dynamic-slice_convert_fusion.2), channel_id=1, source_target_pairs={{0,2},{1,3},{2,0},{3,1},{4,6},{5,7},{6,4},{7,5},{8,10},{9,11},{10,... | collective-permute-start | bytes 1572872 | tf_op jit(solution)/shard_map/ppermute | solution.py:23
  446.9 1.3 copy-start.7
  449.1 21.6 %collective-permute-start.15 = (bf16[1,256,1024]{2,1,0:T(8,128)(2,1)}, bf16[1,256,1024]{2,1,0:T(8,128)(2,1)}, u32[]{:S(2)}, u32[]{:S(2)}) collective-permute-start(bf16[1,256,1024]{2,1,0:T(8,128)(2,1)} %dynamic-slice_convert_fusion.3), channel_id=1, source_target_pairs={{0,2},{1,3},{2,0},{3,1},{4,6},{5,7},{6,4},{7,5},{8,10},{9,11},{10,... | collective-permute-start | bytes 1572872 | tf_op jit(solution)/shard_map/ppermute | solution.py:23
  473.9 1.7 copy-start.11
  478.7 1.0 copy-start.4
  479.8 24.8 %collective-permute-start.18 = (bf16[1,256,2,1024]{1,3,2,0:T(8,128)(2,1)S(1)}, bf16[1,256,2,1024]{1,3,2,0:T(8,128)(2,1)S(1)}, u32[]{:S(2)}, u32[]{:S(2)}) collective-permute-start(bf16[1,256,2,1024]{1,3,2,0:T(8,128)(2,1)S(1)} %maximum_bitcast_fusion.5), channel_id=1, source_target_pairs={{0,2},{1,3},{2,0},{3,1},{4,6},{5,7},{6,4},{7,5},{8,10},{9,11},{10,... | collective-permute-start | bytes 3145736 | tf_op jit(solution)/shard_map/ppermute | solution.py:23
  506.2 4.5 collective-permute-start.19
  506.2 64.3 %collective-permute-start.20 = (bf16[1024,1376]{0,1:T(8,128)(2,1)}, bf16[1024,1376]{0,1:T(8,128)(2,1)}, u32[]{:S(2)}, u32[]{:S(2)}) collective-permute-start(bf16[1024,1376]{0,1:T(8,128)(2,1)} %all-gather.22.cloned.1.call-done), channel_id=1, source_target_pairs={{0,4},{4,0},{8,12},{12,8},{16,20},{20,16},{24,28},{28,24},{1,5},{5... | collective-permute-start | bytes 8454152 | tf_op jit(solution)/shard_map/ppermute | solution.py:23
  507.9 122.9 %collective-permute-start.21 = (bf16[1024,1376]{0,1:T(8,128)(2,1)}, bf16[1024,1376]{0,1:T(8,128)(2,1)}, u32[]{:S(2)}, u32[]{:S(2)}) collective-permute-start(bf16[1024,1376]{0,1:T(8,128)(2,1)} %all-gather.24.cloned.1.call-done), channel_id=1, source_target_pairs={{0,4},{4,0},{8,12},{12,8},{16,20},{20,16},{24,28},{28,24},{1,5},{5... | collective-permute-start | bytes 8454152 | tf_op jit(solution)/shard_map/ppermute | solution.py:23
  508.2 182.6 %collective-permute-start.22 = (bf16[1376,1024]{1,0:T(8,128)(2,1)}, bf16[1376,1024]{1,0:T(8,128)(2,1)}, u32[]{:S(2)}, u32[]{:S(2)}) collective-permute-start(bf16[1376,1024]{1,0:T(8,128)(2,1)} %all-gather.26.cloned.1.call-done), channel_id=1, source_target_pairs={{0,4},{4,0},{8,12},{12,8},{16,20},{20,16},{24,28},{28,24},{1,5},{5... | collective-permute-start | bytes 8454152 | tf_op jit(solution)/shard_map/ppermute | solution.py:23
  514.9 6.7 copy-start.23
  521.6 4.9 copy-start.10
  521.6 4.9 copy-start.24
  659.8 5.1 copy-start.13
  664.9 30.9 %copy-start.2 = (bf16[2,1,1,256,1376]{3,1,0,4,2:T(2,128)(2,1)S(1)}, bf16[2,1,1,256,1376]{3,1,0,4,2:T(2,128)(2,1)}, u32[]{:S(2)}) copy-start(bf16[2,1,1,256,1376]{3,1,0,4,2:T(2,128)(2,1)} %get-tuple-element.22) | copy-start | bytes 4227076
  664.9 44.3 %collective-permute-start.25 = (bf16[2,256,1024]{2,1,0:T(8,128)(2,1)}, bf16[2,256,1024]{2,1,0:T(8,128)(2,1)}, u32[]{:S(2)}, u32[]{:S(2)}) collective-permute-start(bf16[2,256,1024]{2,1,0:T(8,128)(2,1)} %bitcast.63), channel_id=1, source_target_pairs={{0,1},{1,0},{2,3},{3,2},{4,5},{5,4},{6,7},{7,6},{8,9},{9,8},{10,11... | collective-permute-start | bytes 3145736 | tf_op jit(solution)/shard_map/ppermute | solution.py:23
  701.4 11.3 %collective-permute-start.23 = (bf16[2,256,1024]{2,1,0:T(8,128)(2,1)}, bf16[2,256,1024]{2,1,0:T(8,128)(2,1)S(1)}, u32[]{:S(2)}, u32[]{:S(2)}) collective-permute-start(bf16[2,256,1024]{2,1,0:T(8,128)(2,1)} %bitcast.238), channel_id=1, source_target_pairs={{0,1},{1,0},{2,3},{3,2},{4,5},{5,4},{6,7},{7,6},{8,9},{9,8},{10,11... | collective-permute-start | bytes 3145736 | tf_op jit(solution)/shard_map/ppermute | solution.py:23
  701.4 4.1 copy-start.15
  710.9 14.9 %collective-permute-start.26 = (bf16[1,256,1024]{2,1,0:T(8,128)(2,1)S(1)}, bf16[1,256,1024]{2,1,0:T(8,128)(2,1)S(1)}, u32[]{:S(2)}, u32[]{:S(2)}) collective-permute-start(bf16[1,256,1024]{2,1,0:T(8,128)(2,1)S(1)} %dynamic-slice_convert_fusion), channel_id=1, source_target_pairs={{0,2},{1,3},{2,0},{3,1},{4,6},{5,7},{6,4},{7,5},{8,10},{9,11},{10,... | collective-permute-start | bytes 1572872 | tf_op jit(solution)/shard_map/ppermute | solution.py:23
  713.2 23.4 %collective-permute-start.24 = (bf16[1,256,1024]{2,1,0:T(8,128)(2,1)S(1)}, bf16[1,256,1024]{2,1,0:T(8,128)(2,1)S(1)}, u32[]{:S(2)}, u32[]{:S(2)}) collective-permute-start(bf16[1,256,1024]{2,1,0:T(8,128)(2,1)S(1)} %dynamic-slice_convert_fusion.1), channel_id=1, source_target_pairs={{0,2},{1,3},{2,0},{3,1},{4,6},{5,7},{6,4},{7,5},{8,10},{9,11},{10,... | collective-permute-start | bytes 1572872 | tf_op jit(solution)/shard_map/ppermute | solution.py:23
  737.6 1.2 copy-start.5
  (2 other events, 1.4 us)
Sparse Core Ops, SparseCore 0:
  8.9 60.7 all-gather.9
  71.2 56.2 all-gather.11
  129.1 56.2 all-gather.13
  186.8 35.1 all-gather.17
  223.4 35.8 all-gather.15
  260.8 36.5 all-gather.19
  298.9 56.2 all-gather.21
  356.8 56.2 all-gather.23
  449.5 56.4 all-gather.25
